TPU v7x, 32 devices: a whole 2x2x4 slice. The times are simulated.
32 devices in a mesh: ep: 8 (over z, x), tp: 4 (over y, core).
Axes of the slice: x: 2, y: 2, z: 4, core: 2. Of those that a mesh axis runs over, the one named last changes fastest.
Arguments:
- queries: bfloat16 [6144, 1024], P('ep', 'tp'), may hold values from -6.5 to 6.5
- keys: bfloat16 [6144, 1024], P('ep', 'tp'), may hold values from -6.5 to 6.5
- values: bfloat16 [6144, 1024], P('ep', 'tp'), may hold values from -6 to 6
- cum_gate: float32 [6144, 16], P('ep', 'tp'), may hold values from -770 to 0, as said below
- head_gain: float32 [1024], P('tp'), may hold values from 0.1 to 1.9
- moe_in: bfloat16 [1024, 2048], P('ep'), may hold values from -6 to 6
- ffn_gain: float32 [2048], replicated, may hold values from 0.1 to 1.9
- routes: int32 [1024, 4], P('ep'), may hold values from 0 to 31, all different within a row; in each aligned block of 128 rows (0 to 127, 128 to 255, ...) at most 24 rows name the same one
- route_weight: float32 [1024, 4], P('ep'), may hold values from 0.2 to 1.2
- expert_gate: bfloat16 [32, 1024, 2048], P('ep', 'tp'), may hold values from -0.125 to 0.125
- expert_up: bfloat16 [32, 1024, 2048], P('ep', 'tp'), may hold values from -0.125 to 0.125
- expert_down: bfloat16 [32, 1024, 2048], P('ep', 'tp'), may hold values from -0.25 to 0.25
- shared_gate: bfloat16 [512, 2048], P('tp'), may hold values from -0.125 to 0.125
- shared_up: bfloat16 [512, 2048], P('tp'), may hold values from -0.125 to 0.125
- shared_down: bfloat16 [512, 2048], P('tp'), may hold values from -0.375 to 0.375
Outputs:
- mixed: bfloat16 [6144, 1024], P('ep', 'tp')
- expert_out: bfloat16 [1024, 2048], P('ep', 'tp')
Inputs may be any that keep to these rules, and one draw needn't show every extreme that they name: `routes`: in each aligned block of 128 rows (the tokens of one index of ep) no expert is named by more than 24 rows, a bound that some block reaches; a row names 4 different experts. Each head's cum_gate never rises from one position to the next.
All inputs are finite; a program needn't handle non-finite values.
Results may differ from a plain program's by a relative error of at most 0.019.
Values may be sent and summed in bfloat16 or wider, within the bound.
A program may use at most 128 MiB of HBM per device.

v0:
```python
import math
import jax
import jax.numpy as jnp
from jax import lax
from jax.sharding import PartitionSpec as P

NORM_EPSILON = 1e-06


def keep_same(state_pair):
    return state_pair


def attend(queries, keys, values, cum_gate, head_gain):
    row_count, head_width = queries.shape
    head_count = cum_gate.shape[1]
    head_size = head_width // head_count
    score_scale = head_size ** (-0.5)
    first_row = lax.axis_index("ep") * row_count
    last_row = first_row + row_count - 1
    query_heads = queries.reshape(row_count, head_count, head_size)
    query_pos = first_row + jnp.arange(row_count, dtype=jnp.int32)
    query_gate = cum_gate.T
    all_gates = lax.all_gather(cum_gate, "ep", axis=0, tiled=True)
    start_state = (
        jnp.full((head_count, row_count), -1e30, jnp.float32),
        jnp.zeros((row_count, head_count, head_size), jnp.float32),
    )
    key_piece = lax.all_gather(keys, "ep", axis=0, tiled=True)
    value_piece = lax.all_gather(values, "ep", axis=0, tiled=True)
    piece_len = key_piece.shape[0]
    block_len = math.gcd(piece_len, 512)

    def visit(block_num, state_pair):
        offset = block_num * block_len

        def update(pair_in):
            running, weighted = pair_in
            key_block = lax.dynamic_slice_in_dim(key_piece, offset, block_len, 0).reshape(
                block_len, head_count, head_size
            )
            value_block = lax.dynamic_slice_in_dim(value_piece, offset, block_len, 0).reshape(
                block_len, head_count, head_size
            )
            key_gate = lax.dynamic_slice_in_dim(all_gates, offset, block_len, 0).T
            key_pos = offset + jnp.arange(block_len, dtype=jnp.int32)
            scores = (
                jnp.einsum(
                    "qhd,khd->hqk", query_heads, key_block, preferred_element_type=jnp.float32
                )
                * score_scale
            )
            scores = scores + query_gate[:, :, None] - key_gate[:, None, :]
            scores = jnp.where(key_pos[None, None, :] <= query_pos[None, :, None], scores, -jnp.inf)
            new_peak = jnp.maximum(running, jnp.max(scores, axis=2))
            weights = jnp.exp(scores - new_peak[:, :, None]).astype(jnp.bfloat16)
            shrink = jnp.exp(running - new_peak).T
            weighted = weighted * shrink[:, :, None] + jnp.einsum(
                "hqk,khd->qhd", weights, value_block, preferred_element_type=jnp.float32
            )
            return (new_peak, weighted)

        return lax.cond(offset <= last_row, update, keep_same, state_pair)

    running, weighted = lax.fori_loop(0, piece_len // block_len, visit, start_state)
    mean_square = jnp.mean(weighted * weighted, axis=2, keepdims=True)
    normed = (
        weighted * lax.rsqrt(mean_square + NORM_EPSILON) * head_gain.reshape(head_count, head_size)
    )
    return normed.reshape(row_count, head_width).astype(jnp.bfloat16)


def slot_index(route_rows, experts, capacity):
    flat_routes = route_rows.reshape(-1)
    agreement_tally = (
        flat_routes[:, None] == jnp.arange(experts, dtype=jnp.int32)[None, :]
    ).astype(jnp.int32)
    earlier = jnp.sum((jnp.cumsum(agreement_tally, axis=0) - 1) * agreement_tally, axis=1)
    return flat_routes * capacity + earlier


def experts_half(
    moe_in,
    ffn_gain,
    routes,
    route_weight,
    expert_gate,
    expert_up,
    expert_down,
    shared_gate,
    shared_up,
    shared_down,
):
    tokens, model_width = moe_in.shape
    choose = routes.shape[1]
    per_group = expert_gate.shape[0]
    groups = lax.axis_size("ep")
    experts = per_group * groups
    capacity = max(2, 3 * tokens * choose // (2 * experts))
    slice_width = model_width // lax.axis_size("tp")
    source = moe_in.astype(jnp.float32)
    normed = (
        source
        * lax.rsqrt(jnp.mean(source * source, axis=1, keepdims=True) + NORM_EPSILON)
        * ffn_gain
    ).astype(jnp.bfloat16)
    shared_hidden = (
        jax.nn.silu(
            jnp.einsum("td,fd->tf", normed, shared_gate, preferred_element_type=jnp.float32)
        )
        * jnp.einsum("td,fd->tf", normed, shared_up, preferred_element_type=jnp.float32)
    ).astype(jnp.bfloat16)
    shared_term = jnp.dot(shared_hidden, shared_down, preferred_element_type=jnp.float32)
    slot_ids = slot_index(routes, experts, capacity)
    owner_row = (
        jnp.full((experts * capacity,), tokens, jnp.int32)
        .at[slot_ids]
        .set(jnp.arange(tokens * choose, dtype=jnp.int32) // choose)
    )
    padded = jnp.concatenate([normed, jnp.zeros((1, model_width), normed.dtype)], axis=0)
    own_columns = lax.dynamic_slice_in_dim(
        padded, lax.axis_index("tp") * slice_width, slice_width, 1
    )
    arrived = lax.all_to_all(own_columns[owner_row], "ep", split_axis=0, concat_axis=0, tiled=True)
    column_piece = lax.all_gather(arrived, "tp", axis=1, tiled=True)
    piece_len = column_piece.shape[1]
    arranged = column_piece.reshape(groups, per_group, capacity, piece_len)
    gate_value = jnp.einsum(
        "slcd,lfd->slcf", arranged, expert_gate, preferred_element_type=jnp.float32
    )
    up_value = jnp.einsum("slcd,lfd->slcf", arranged, expert_up, preferred_element_type=jnp.float32)
    hidden = (jax.nn.silu(gate_value) * up_value).astype(jnp.bfloat16)
    expert_term = jnp.einsum(
        "slcf,lfd->slcd", hidden, expert_down, preferred_element_type=jnp.float32
    ).reshape(groups * per_group * capacity, model_width)
    expert_sum, shared_sum = (
        lax.psum_scatter(
            expert_term.astype(jnp.bfloat16), "tp", scatter_dimension=1, tiled=True
        ).astype(jnp.float32),
        lax.psum_scatter(
            shared_term.astype(jnp.bfloat16), "tp", scatter_dimension=1, tiled=True
        ).astype(jnp.float32),
    )
    returned = lax.all_to_all(
        expert_sum.astype(jnp.bfloat16), "ep", split_axis=0, concat_axis=0, tiled=True
    )
    picked = returned[slot_ids].reshape(tokens, choose, slice_width).astype(jnp.float32)
    routed = jnp.sum(picked * route_weight[:, :, None], axis=1)
    return (shared_sum + routed).astype(jnp.bfloat16)


def on_device(
    queries,
    keys,
    values,
    cum_gate,
    head_gain,
    moe_in,
    ffn_gain,
    routes,
    route_weight,
    expert_gate,
    expert_up,
    expert_down,
    shared_gate,
    shared_up,
    shared_down,
):
    mixed = attend(queries, keys, values, cum_gate, head_gain)
    expert_out = experts_half(
        moe_in,
        ffn_gain,
        routes,
        route_weight,
        expert_gate,
        expert_up,
        expert_down,
        shared_gate,
        shared_up,
        shared_down,
    )
    return (mixed, expert_out)


def solution(mesh):
    in_specs = (
        P("ep", "tp"),
        P("ep", "tp"),
        P("ep", "tp"),
        P("ep", "tp"),
        P("tp"),
        P("ep", None),
        P(),
        P("ep", None),
        P("ep", None),
        P("ep", "tp", None),
        P("ep", "tp", None),
        P("ep", "tp", None),
        P("tp", None),
        P("tp", None),
        P("tp", None),
    )
    out_specs = (P("ep", "tp"), P("ep", "tp"))
    return jax.shard_map(
        on_device, mesh=mesh, in_specs=in_specs, out_specs=out_specs, check_vma=False
    )
```

profile of v0, /device:TPU:27, one launch (start us, length us, event | category | flops | bytes accessed | tf_op | source)
XLA Modules:
  0.0 309.0 jit_solution(3351411150945842040)
XLA Ops:
  9.8 1.2 fusion.44
  11.3 1.2 reduce-window.6
  12.8 2.4 scatter_custom_fusion
  15.3 1.2 fusion.46
  16.6 2.7 gather_fusion
  19.3 23.3 %all_to_all.24 = bf16[8,96,512]{2,1,0:T(8,128)(2,1)} all-to-all(bf16[8,96,512]{2,1,0:T(8,128)(2,1)S(1)} %bitcast.100), channel_id=1, replica_groups=mesh['ep'=8,'tp'=4] {'ep'}, dimensions={0} | all-to-all | bytes 1572864 | tf_op jit(solution)/shard_map/all_to_all | solution.py:124
  42.6 30.3 %all-gather.8.cloned.1.call-done = bf16[768,2048]{1,0:T(8,128)(2,1)} async-done(((bf16[768,512]{1,0:T(8,128)(2,1)}), bf16[768,2048]{1,0:T(8,128)(2,1)}) %all-gather.8.cloned.1.call-update) | async-done | bytes 3145744 | tf_op jit(solution)/shard_map/all_gather | solution.py:125
  73.0 4.7 %fusion.23 = f32[8,4,24,256]{3,2,0,1:T(8,128)S(1)} fusion(bf16[4,256,2048]{2,1,0:T(8,128)(2,1)} %param.28, bf16[8,4,24,2048]{3,2,1,0:T(8,128)(2,1)} %bitcast.109), kind=kOutput, calls=%fused_computation.33 | convolution fusion | flops 805306368 | bytes 8126464 | tf_op jit(solution)/shard_map/slcd,lfd->slcf/dot_general | solution.py:128
  77.6 8.5 %fusion.18 = bf16[8,4,24,2048]{3,2,0,1:T(8,128)(2,1)} fusion(bf16[4,256,2048]{2,1,0:T(8,128)(2,1)} %param.30, bf16[4,256,2048]{2,1,0:T(8,128)(2,1)} %param.29, bf16[8,4,24,2048]{3,2,1,0:T(8,128)(2,1)} %bitcast.110, f32[8,4,24,256]{3,2,0,1:T(8,128)S(1)} %fusion.23), kind=kOutput, calls=%fused_computation.27 | convolution fusion | flops 1613365248 | bytes 15466496 | tf_op jit(solution)/shard_map/slcf,lfd->slcd/dot_general | solution.py:133
  86.1 4.1 %copy.32 = bf16[8,4,24,2048]{3,2,1,0:T(8,128)(2,1)} copy(bf16[8,4,24,2048]{3,2,0,1:T(8,128)(2,1)} %fusion.18) | data formatting | bytes 6291456 | tf_op jit(solution)/shard_map/convert_element_type | solution.py:138
  92.3 35.2 %reduce-scatter.5.cloned.1.call-done = bf16[768,512]{1,0:T(8,128)(2,1)} async-done(((bf16[768,2048]{1,0:T(8,128)(2,1)}), bf16[768,512]{1,0:T(8,128)(2,1)}) %reduce-scatter.5.cloned.1.call-update) | async-done | bytes 786448 | tf_op jit(solution)/shard_map/reduce_scatter | solution.py:137
  127.5 5.4 %all-to-all-start.1 = ((bf16[8,96,512]{2,1,0:T(8,128)(2,1)}), bf16[8,96,512]{2,1,0:T(8,128)(2,1)S(1)}, u32[]{:S(2)}, u32[]{:S(2)}) async-start(bf16[8,96,512]{2,1,0:T(8,128)(2,1)} %bitcast.103), calls=%async_computation.3 | async-start | bytes 1572864 | tf_op jit(solution)/shard_map/all_to_all | solution.py:144
  133.3 1.6 convolution_convert_fusion
  135.3 44.6 %all_gather.13 = f32[6144,4]{0,1:T(4,128)S(1)} all-gather(f32[768,4]{0,1:T(4,128)S(1)} %copy-done.6), channel_id=1, replica_groups=mesh['ep'=8,'tp'=4] {'ep'}, dimensions={0}, use_global_device_ids=true | all-gather | bytes 110592 | tf_op jit(solution)/shard_map/all_gather | solution.py:24
  179.9 46.6 %all-gather.6.cloned.1.call-done = bf16[6144,256]{0,1:T(8,128)(2,1)} async-done(((bf16[768,256]{0,1:T(8,128)(2,1)}), bf16[6144,256]{0,1:T(8,128)(2,1)}) %all-gather.6.cloned.1.call-update) | async-done | bytes 3145744 | tf_op jit(solution)/shard_map/all_gather | solution.py:30
  226.6 69.5 %while.16 = (s32[]{:T(128)}, f32[4,768]{1,0:T(4,128)S(1)}, f32[768,4,64]{0,2,1:T(8,128)S(1)}, s32[]{:T(128)}, bf16[6144,256]{0,1:T(8,128)(2,1)}, /*index=5*/bf16...) while((s32[]{:T(128)}, f32[4,768]{1,0:T(4,128)S(1)}, ...), condition=%wide.region_4.5_spmd.clone, body=%wide.region_0.4_spmd.clone.sunk | while | flops 420745472 | bytes 17461568 | solution.py:65
  226.7 5.8 %conditional.3 = ((f32[4,768]{1,0:T(4,128)S(1)}, f32[768,4,64]{0,2,1:T(8,128)S(1)})) conditional(s32[]{:T(128)} %convert_element_type.106, (f32[4,768]{1,0:T(4,128)S(1)}, f32[768,4,64]{0,2,1:T(8,128)S(1)}) %tuple.50, (s32[]{:T(128)}, s32[]{:T(128)}, bf16[6144,256]{0,1:T(8,128)(2,1)}, bf16[768,4,64]{0,2,1:T(8,128)(2,1)S(1)}, f32[4,768]{1,0:T(4,128)S(1)}, ...), branch_computations={%region_1.0_spmd, %region_2.3_spmd} | conditional | flops 420745472 | bytes 17458250 | solution.py:63
  227.0 1.1 constant_dynamic-slice_fusion
  228.1 1.9 fusion.2
  230.0 2.4 fusion.6
  232.5 5.7 %conditional.3 = ((f32[4,768]{1,0:T(4,128)S(1)}, f32[768,4,64]{0,2,1:T(8,128)S(1)})) conditional(s32[]{:T(128)} %convert_element_type.106, (f32[4,768]{1,0:T(4,128)S(1)}, f32[768,4,64]{0,2,1:T(8,128)S(1)}) %tuple.50, (s32[]{:T(128)}, s32[]{:T(128)}, bf16[6144,256]{0,1:T(8,128)(2,1)}, bf16[768,4,64]{0,2,1:T(8,128)(2,1)S(1)}, f32[4,768]{1,0:T(4,128)S(1)}, ...), branch_computations={%region_1.0_spmd, %region_2.3_spmd} | conditional | flops 420745472 | bytes 17458250 | solution.py:63
  232.8 1.1 constant_dynamic-slice_fusion
  233.9 1.9 fusion.2
  235.8 2.4 fusion.6
  238.3 5.7 %conditional.3 = ((f32[4,768]{1,0:T(4,128)S(1)}, f32[768,4,64]{0,2,1:T(8,128)S(1)})) conditional(s32[]{:T(128)} %convert_element_type.106, (f32[4,768]{1,0:T(4,128)S(1)}, f32[768,4,64]{0,2,1:T(8,128)S(1)}) %tuple.50, (s32[]{:T(128)}, s32[]{:T(128)}, bf16[6144,256]{0,1:T(8,128)(2,1)}, bf16[768,4,64]{0,2,1:T(8,128)(2,1)S(1)}, f32[4,768]{1,0:T(4,128)S(1)}, ...), branch_computations={%region_1.0_spmd, %region_2.3_spmd} | conditional | flops 420745472 | bytes 17458250 | solution.py:63
  238.6 1.1 constant_dynamic-slice_fusion
  239.7 1.9 fusion.2
  241.6 2.4 fusion.6
  244.0 5.7 %conditional.3 = ((f32[4,768]{1,0:T(4,128)S(1)}, f32[768,4,64]{0,2,1:T(8,128)S(1)})) conditional(s32[]{:T(128)} %convert_element_type.106, (f32[4,768]{1,0:T(4,128)S(1)}, f32[768,4,64]{0,2,1:T(8,128)S(1)}) %tuple.50, (s32[]{:T(128)}, s32[]{:T(128)}, bf16[6144,256]{0,1:T(8,128)(2,1)}, bf16[768,4,64]{0,2,1:T(8,128)(2,1)S(1)}, f32[4,768]{1,0:T(4,128)S(1)}, ...), branch_computations={%region_1.0_spmd, %region_2.3_spmd} | conditional | flops 420745472 | bytes 17458250 | solution.py:63
  244.4 1.1 constant_dynamic-slice_fusion
  245.5 1.9 fusion.2
  247.4 2.4 fusion.6
  249.8 5.7 %conditional.3 = ((f32[4,768]{1,0:T(4,128)S(1)}, f32[768,4,64]{0,2,1:T(8,128)S(1)})) conditional(s32[]{:T(128)} %convert_element_type.106, (f32[4,768]{1,0:T(4,128)S(1)}, f32[768,4,64]{0,2,1:T(8,128)S(1)}) %tuple.50, (s32[]{:T(128)}, s32[]{:T(128)}, bf16[6144,256]{0,1:T(8,128)(2,1)}, bf16[768,4,64]{0,2,1:T(8,128)(2,1)S(1)}, f32[4,768]{1,0:T(4,128)S(1)}, ...), branch_computations={%region_1.0_spmd, %region_2.3_spmd} | conditional | flops 420745472 | bytes 17458250 | solution.py:63
  250.2 1.1 constant_dynamic-slice_fusion
  251.3 1.9 fusion.2
  253.2 2.4 fusion.6
  255.6 5.7 %conditional.3 = ((f32[4,768]{1,0:T(4,128)S(1)}, f32[768,4,64]{0,2,1:T(8,128)S(1)})) conditional(s32[]{:T(128)} %convert_element_type.106, (f32[4,768]{1,0:T(4,128)S(1)}, f32[768,4,64]{0,2,1:T(8,128)S(1)}) %tuple.50, (s32[]{:T(128)}, s32[]{:T(128)}, bf16[6144,256]{0,1:T(8,128)(2,1)}, bf16[768,4,64]{0,2,1:T(8,128)(2,1)S(1)}, f32[4,768]{1,0:T(4,128)S(1)}, ...), branch_computations={%region_1.0_spmd, %region_2.3_spmd} | conditional | flops 420745472 | bytes 17458250 | solution.py:63
  256.0 1.1 constant_dynamic-slice_fusion
  257.1 1.9 fusion.2
  259.0 2.4 fusion.6
  261.4 5.7 %conditional.3 = ((f32[4,768]{1,0:T(4,128)S(1)}, f32[768,4,64]{0,2,1:T(8,128)S(1)})) conditional(s32[]{:T(128)} %convert_element_type.106, (f32[4,768]{1,0:T(4,128)S(1)}, f32[768,4,64]{0,2,1:T(8,128)S(1)}) %tuple.50, (s32[]{:T(128)}, s32[]{:T(128)}, bf16[6144,256]{0,1:T(8,128)(2,1)}, bf16[768,4,64]{0,2,1:T(8,128)(2,1)S(1)}, f32[4,768]{1,0:T(4,128)S(1)}, ...), branch_computations={%region_1.0_spmd, %region_2.3_spmd} | conditional | flops 420745472 | bytes 17458250 | solution.py:63
  261.8 1.1 constant_dynamic-slice_fusion
  262.9 1.9 fusion.2
  264.8 2.4 fusion.6
  267.2 5.7 %conditional.3 = ((f32[4,768]{1,0:T(4,128)S(1)}, f32[768,4,64]{0,2,1:T(8,128)S(1)})) conditional(s32[]{:T(128)} %convert_element_type.106, (f32[4,768]{1,0:T(4,128)S(1)}, f32[768,4,64]{0,2,1:T(8,128)S(1)}) %tuple.50, (s32[]{:T(128)}, s32[]{:T(128)}, bf16[6144,256]{0,1:T(8,128)(2,1)}, bf16[768,4,64]{0,2,1:T(8,128)(2,1)S(1)}, f32[4,768]{1,0:T(4,128)S(1)}, ...), branch_computations={%region_1.0_spmd, %region_2.3_spmd} | conditional | flops 420745472 | bytes 17458250 | solution.py:63
  267.6 1.1 constant_dynamic-slice_fusion
  268.6 1.9 fusion.2
  270.6 2.4 fusion.6
  273.0 5.7 %conditional.3 = ((f32[4,768]{1,0:T(4,128)S(1)}, f32[768,4,64]{0,2,1:T(8,128)S(1)})) conditional(s32[]{:T(128)} %convert_element_type.106, (f32[4,768]{1,0:T(4,128)S(1)}, f32[768,4,64]{0,2,1:T(8,128)S(1)}) %tuple.50, (s32[]{:T(128)}, s32[]{:T(128)}, bf16[6144,256]{0,1:T(8,128)(2,1)}, bf16[768,4,64]{0,2,1:T(8,128)(2,1)S(1)}, f32[4,768]{1,0:T(4,128)S(1)}, ...), branch_computations={%region_1.0_spmd, %region_2.3_spmd} | conditional | flops 420745472 | bytes 17458250 | solution.py:63
  273.4 1.1 constant_dynamic-slice_fusion
  274.4 1.9 fusion.2
  276.4 2.4 fusion.6
  278.8 5.7 %conditional.3 = ((f32[4,768]{1,0:T(4,128)S(1)}, f32[768,4,64]{0,2,1:T(8,128)S(1)})) conditional(s32[]{:T(128)} %convert_element_type.106, (f32[4,768]{1,0:T(4,128)S(1)}, f32[768,4,64]{0,2,1:T(8,128)S(1)}) %tuple.50, (s32[]{:T(128)}, s32[]{:T(128)}, bf16[6144,256]{0,1:T(8,128)(2,1)}, bf16[768,4,64]{0,2,1:T(8,128)(2,1)S(1)}, f32[4,768]{1,0:T(4,128)S(1)}, ...), branch_computations={%region_1.0_spmd, %region_2.3_spmd} | conditional | flops 420745472 | bytes 17458250 | solution.py:63
  280.2 1.9 fusion.2
  282.1 2.4 fusion.6
  284.6 5.7 %conditional.3 = ((f32[4,768]{1,0:T(4,128)S(1)}, f32[768,4,64]{0,2,1:T(8,128)S(1)})) conditional(s32[]{:T(128)} %convert_element_type.106, (f32[4,768]{1,0:T(4,128)S(1)}, f32[768,4,64]{0,2,1:T(8,128)S(1)}) %tuple.50, (s32[]{:T(128)}, s32[]{:T(128)}, bf16[6144,256]{0,1:T(8,128)(2,1)}, bf16[768,4,64]{0,2,1:T(8,128)(2,1)S(1)}, f32[4,768]{1,0:T(4,128)S(1)}, ...), branch_computations={%region_1.0_spmd, %region_2.3_spmd} | conditional | flops 420745472 | bytes 17458250 | solution.py:63
  286.0 1.9 fusion.2
  287.9 2.4 fusion.6
  290.4 5.7 %conditional.3 = ((f32[4,768]{1,0:T(4,128)S(1)}, f32[768,4,64]{0,2,1:T(8,128)S(1)})) conditional(s32[]{:T(128)} %convert_element_type.106, (f32[4,768]{1,0:T(4,128)S(1)}, f32[768,4,64]{0,2,1:T(8,128)S(1)}) %tuple.50, (s32[]{:T(128)}, s32[]{:T(128)}, bf16[6144,256]{0,1:T(8,128)(2,1)}, bf16[768,4,64]{0,2,1:T(8,128)(2,1)S(1)}, f32[4,768]{1,0:T(4,128)S(1)}, ...), branch_computations={%region_1.0_spmd, %region_2.3_spmd} | conditional | flops 420745472 | bytes 17458250 | solution.py:63
  290.7 1.1 constant_dynamic-slice_fusion
  291.8 1.9 fusion.2
  293.7 2.4 fusion.6
  297.3 2.0 gather_fusion.1
  300.3 1.6 add_convert_fusion
  (137 shorter events, 13.5 us)
Async XLA Ops:
  8.0 125.3 %copy-start = (bf16[128,2048]{1,0:T(8,128)(2,1)S(1)}, bf16[128,2048]{1,0:T(8,128)(2,1)}, u32[]{:S(2)}) copy-start(bf16[128,2048]{1,0:T(8,128)(2,1)} %param.33) | copy-start | bytes 1572868
  8.0 65.0 %all-gather.8.cloned.1.call-start = ((), (), s32[]{:S(2)}) async-start(), calls=%async_computation.7 | async-start | bytes 3932160 | tf_op jit(solution)/shard_map/all_gather | solution.py:125
  42.6 84.9 %reduce-scatter.5.cloned.1.call-start = ((), (), s32[]{:S(2)}) async-start(), calls=%async_computation.8 | async-start | bytes 3932160 | tf_op jit(solution)/shard_map/reduce_scatter | solution.py:137
  86.1 4.2 %copy-start.3 = (bf16[768,256]{1,0:T(8,128)(2,1)S(1)}, bf16[768,256]{1,0:T(8,128)(2,1)}, u32[]{:S(2)}) copy-start(bf16[768,256]{1,0:T(8,128)(2,1)} %param.20) | copy-start | bytes 1179652
  86.1 5.2 %copy-start.4 = (bf16[768,256]{1,0:T(8,128)(2,1)S(1)}, bf16[768,256]{1,0:T(8,128)(2,1)}, u32[]{:S(2)}) copy-start(bf16[768,256]{1,0:T(8,128)(2,1)} %param.21) | copy-start | bytes 1179652
  90.2 42.8 %copy-start.1 = (bf16[128,2048]{1,0:T(8,128)(2,1)S(1)}, bf16[128,2048]{1,0:T(8,128)(2,1)}, u32[]{:S(2)}) copy-start(bf16[128,2048]{1,0:T(8,128)(2,1)} %param.31) | copy-start | bytes 1572868
  90.2 43.1 %copy-start.2 = (bf16[128,2048]{1,0:T(8,128)(2,1)S(1)}, bf16[128,2048]{1,0:T(8,128)(2,1)}, u32[]{:S(2)}) copy-start(bf16[128,2048]{1,0:T(8,128)(2,1)} %param.32) | copy-start | bytes 1572868
  90.2 44.7 %copy-start.5 = (bf16[768,256]{1,0:T(8,128)(2,1)S(1)}, bf16[768,256]{1,0:T(8,128)(2,1)}, u32[]{:S(2)}) copy-start(bf16[768,256]{1,0:T(8,128)(2,1)} %param.19) | copy-start | bytes 1179652
  90.2 44.8 %copy-start.8 = (f32[256]{0:T(256)S(1)}, f32[256]{0:T(256)}, u32[]{:S(2)}) copy-start(f32[256]{0:T(256)} %param.23) | copy-start | bytes 3076
  90.3 44.9 %copy-start.7 = (f32[128,4]{0,1:T(4,128)S(1)}, f32[128,4]{0,1:T(4,128)}, u32[]{:S(2)}) copy-start(f32[128,4]{0,1:T(4,128)} %param.27) | copy-start | bytes 6148
  90.3 45.0 %copy-start.6 = (f32[768,4]{0,1:T(4,128)S(1)}, f32[768,4]{0,1:T(4,128)}, u32[]{:S(2)}) copy-start(f32[768,4]{0,1:T(4,128)} %param.22) | copy-start | bytes 36868
  90.3 89.6 %all-gather.4.cloned.1.call-start = ((), (), s32[]{:S(2)}) async-start(), calls=%async_computation.4 | async-start | bytes 3538944 | tf_op jit(solution)/shard_map/all_gather | solution.py:29
  91.3 135.3 %all-gather.6.cloned.1.call-start = ((), (), s32[]{:S(2)}) async-start(), calls=%async_computation.5 | async-start | bytes 3538944 | tf_op jit(solution)/shard_map/all_gather | solution.py:30
  127.5 169.8 %all-to-all-start.1 = ((bf16[8,96,512]{2,1,0:T(8,128)(2,1)}), bf16[8,96,512]{2,1,0:T(8,128)(2,1)S(1)}, u32[]{:S(2)}, u32[]{:S(2)}) async-start(bf16[8,96,512]{2,1,0:T(8,128)(2,1)} %bitcast.103), calls=%async_computation.3 | async-start | bytes 1572864 | tf_op jit(solution)/shard_map/all_to_all | solution.py:144
  132.9 167.4 %reduce-scatter.3.cloned.1.call-start = ((), (), s32[]{:S(2)}) async-start(), calls=%async_computation.6 | async-start | bytes 655360 | tf_op jit(solution)/shard_map/reduce_scatter | solution.py:140
Sparse Core Ops, SparseCore 0:
  42.7 30.1 all-gather.7
  90.3 37.1 reduce-scatter.4
  136.2 22.2 reduce-scatter.2
Sparse Core Ops, SparseCore 1:
  93.6 71.5 all-gather.3
  167.2 59.4 all-gather.5
where the time goes:
time: 310 us; the launch traced here: 309 us
  waiting for transfers between devices  112 us (36%)
  blocking collectives  67.9 us (22%)
  matrix products  66.4 us (21%)
  local copies, waits for them, and re-layouts  29.2 us (9%)
  between operations  15.5 us (5%)
  other arithmetic  10.8 us (3%)
  starting transfers between devices  5.61 us (2%)
    all_gather x1, waiting for transfers between devices, attend(): value_piece = lax.all_gather(values, 'ep', axis=0, tiled=True)  46.6 us
    all_gather x1, blocking collectives, attend(): all_gates = lax.all_gather(cum_gate, 'ep', axis=0, tiled=True)  44.6 us
    reduce_scatter x1, waiting for transfers between devices, experts_half(): lax.psum_scatter(expert_term.astype(jnp.bfloat16), 'tp', scatter_dimensio...  35.2 us
    all_gather x1, waiting for transfers between devices, experts_half(): column_piece = lax.all_gather(arrived, 'tp', axis=1, tiled=True)  30.3 us
    dot_general x12, matrix products, update(): jnp.einsum('hqk,khd->qhd', weights, value_block, preferred_element_type=j...  28.6 us
    all_to_all x1, blocking collectives, experts_half(): lax.all_to_all(own_columns[owner_row], 'ep', split_axis=0, concat_axis=0,...  23.3 us
    dot_general x12, matrix products, update(): jnp.einsum('qhd,khd->hqk', query_heads, key_block, preferred_element_type...  22.8 us
    dynamic_slice x12, local copies, waits for them, and re-layouts, update(): lax.dynamic_slice_in_dim(value_piece, offset, block_len, 0)  12.9 us
  transfers between devices with their start and end apart: 6, of which 3 were waited for; matrix products, arithmetic and copies ran while one was open for 25% of the time, Pallas kernels for 0%

commit v1 on v0

--- a/solution.py
+++ b/solution.py
@@ -26,8 +26,11 @@
         jnp.full((head_count, row_count), -1e30, jnp.float32),
         jnp.zeros((row_count, head_count, head_size), jnp.float32),
     )
-    key_piece = lax.all_gather(keys, "ep", axis=0, tiled=True)
-    value_piece = lax.all_gather(values, "ep", axis=0, tiled=True)
+    key_piece, value_piece = jnp.split(
+        lax.all_gather(jnp.concatenate([keys, values], 1), "ep", axis=0, tiled=True),
+        [keys.shape[1]],
+        1,
+    )
     piece_len = key_piece.shape[0]
     block_len = math.gcd(piece_len, 512)
 

time: 310 us -> 292 us (0.942)
  blocking collectives: 67.9 us -> 48.9 us
  local copies, waits for them, and re-layouts: 29.2 us -> 34 us
  waiting for transfers between devices: 112 us -> 108 us
    reduce_scatter x1, waiting for transfers between devices: 35.2 us -> 7.8 us  [experts_half(): lax.psum_scatter(expert_term.astype(jnp.bfloat16), 'tp', scatter_dimensio...]
    all_gather x2 -> x1, waiting for transfers between devices: 46.7 us -> 69.7 us  [attend(): lax.all_gather(jnp.concatenate([keys, values], 1), 'ep', axis=0, tiled=True)]
    all_gather x1, blocking collectives: 44.6 us -> 25.6 us  [attend(): all_gates = lax.all_gather(cum_gate, 'ep', axis=0, tiled=True)]
    split x0 -> x1, local copies, waits for them, and re-layouts: none -> 6.25 us  [attend(): jnp.split(lax.all_gather(jnp.concatenate([keys, values], 1), 'ep', axis=0...]
  transfers between devices with their start and end apart: 6 -> 5, of which waited for: 3 -> 3; matrix products, arithmetic and copies ran while one was open for 25% -> 28% of each run, Pallas kernels for 0% -> 0%
where the time goes in v1:
time: 292 us; the launch traced here: 291 us
  waiting for transfers between devices  108 us (37%)
  matrix products  66.4 us (23%)
  blocking collectives  48.9 us (17%)
  local copies, waits for them, and re-layouts  34 us (12%)
  between operations  15.5 us (5%)
  other arithmetic  11.7 us (4%)
  starting transfers between devices  5.6 us (2%)
    all_gather x1, waiting for transfers between devices, attend(): lax.all_gather(jnp.concatenate([keys, values], 1), 'ep', axis=0, tiled=True)  69.7 us
    all_gather x1, waiting for transfers between devices, experts_half(): column_piece = lax.all_gather(arrived, 'tp', axis=1, tiled=True)  30.3 us
    dot_general x12, matrix products, update(): jnp.einsum('hqk,khd->qhd', weights, value_block, preferred_element_type=j...  28.6 us
    all_gather x1, blocking collectives, attend(): all_gates = lax.all_gather(cum_gate, 'ep', axis=0, tiled=True)  25.6 us
    all_to_all x1, blocking collectives, experts_half(): lax.all_to_all(own_columns[owner_row], 'ep', split_axis=0, concat_axis=0,...  23.3 us
    dot_general x12, matrix products, update(): jnp.einsum('qhd,khd->hqk', query_heads, key_block, preferred_element_type...  22.8 us
    dynamic_slice x12, local copies, waits for them, and re-layouts, update(): lax.dynamic_slice_in_dim(value_piece, offset, block_len, 0)  12.9 us
    dot_general x1, matrix products, experts_half(): jnp.einsum('slcf,lfd->slcd', hidden, expert_down, preferred_element_type=...  8.52 us
  transfers between devices with their start and end apart: 5, of which 3 were waited for; matrix products, arithmetic and copies ran while one was open for 28% of the time, Pallas kernels for 0%

profile of v1, /device:TPU:27, one launch (start us, length us, event | category | flops | bytes accessed | tf_op | source)
XLA Modules:
  0.0 291.4 jit_solution(9906781773303249806)
XLA Ops:
  9.8 1.2 fusion.44
  11.3 1.2 reduce-window.6
  12.8 2.4 scatter_custom_fusion
  15.3 1.2 fusion.46
  16.6 2.7 gather_fusion
  19.3 23.3 %all_to_all.24 = bf16[8,96,512]{2,1,0:T(8,128)(2,1)} all-to-all(bf16[8,96,512]{2,1,0:T(8,128)(2,1)S(1)} %bitcast.100), channel_id=1, replica_groups=mesh['ep'=8,'tp'=4] {'ep'}, dimensions={0} | all-to-all | bytes 1572864 | tf_op jit(solution)/shard_map/all_to_all | solution.py:127
  42.6 30.3 %all-gather.5.cloned.1.call-done = bf16[768,2048]{1,0:T(8,128)(2,1)} async-done(((bf16[768,512]{1,0:T(8,128)(2,1)}), bf16[768,2048]{1,0:T(8,128)(2,1)}) %all-gather.5.cloned.1.call-update) | async-done | bytes 3145744 | tf_op jit(solution)/shard_map/all_gather | solution.py:128
  73.0 4.7 %fusion.23 = f32[8,4,24,256]{3,2,0,1:T(8,128)S(1)} fusion(bf16[4,256,2048]{2,1,0:T(8,128)(2,1)} %param.28, bf16[8,4,24,2048]{3,2,1,0:T(8,128)(2,1)} %bitcast.109), kind=kOutput, calls=%fused_computation.33 | convolution fusion | flops 805306368 | bytes 8126464 | tf_op jit(solution)/shard_map/slcd,lfd->slcf/dot_general | solution.py:131
  77.6 8.5 %fusion.18 = bf16[8,4,24,2048]{3,2,0,1:T(8,128)(2,1)} fusion(bf16[4,256,2048]{2,1,0:T(8,128)(2,1)} %param.30, bf16[4,256,2048]{2,1,0:T(8,128)(2,1)} %param.29, bf16[8,4,24,2048]{3,2,1,0:T(8,128)(2,1)} %bitcast.110, f32[8,4,24,256]{3,2,0,1:T(8,128)S(1)} %fusion.23), kind=kOutput, calls=%fused_computation.27 | convolution fusion | flops 1613365248 | bytes 15466496 | tf_op jit(solution)/shard_map/slcf,lfd->slcd/dot_general | solution.py:136
  86.2 4.1 %copy.32 = bf16[8,4,24,2048]{3,2,1,0:T(8,128)(2,1)} copy(bf16[8,4,24,2048]{3,2,0,1:T(8,128)(2,1)} %fusion.18) | data formatting | bytes 6291456 | tf_op jit(solution)/shard_map/convert_element_type | solution.py:141
  92.1 1.6 convolution_convert_fusion
  93.9 25.6 %all_gather.10 = f32[6144,4]{0,1:T(4,128)S(1)} all-gather(f32[768,4]{0,1:T(4,128)S(1)} %copy-done.6), channel_id=1, replica_groups=mesh['ep'=8,'tp'=4] {'ep'}, dimensions={0}, use_global_device_ids=true | all-gather | bytes 110592 | tf_op jit(solution)/shard_map/all_gather | solution.py:24
  119.7 7.8 %reduce-scatter.5.cloned.1.call-done = bf16[768,512]{1,0:T(8,128)(2,1)} async-done(((bf16[768,2048]{1,0:T(8,128)(2,1)}), bf16[768,512]{1,0:T(8,128)(2,1)}) %reduce-scatter.5.cloned.1.call-update) | async-done | bytes 786448 | tf_op jit(solution)/shard_map/reduce_scatter | solution.py:140
  127.5 5.4 %all-to-all-start.1 = ((bf16[8,96,512]{2,1,0:T(8,128)(2,1)}), bf16[8,96,512]{2,1,0:T(8,128)(2,1)S(1)}, u32[]{:S(2)}, u32[]{:S(2)}) async-start(bf16[8,96,512]{2,1,0:T(8,128)(2,1)} %bitcast.103), calls=%async_computation.3 | async-start | bytes 1572864 | tf_op jit(solution)/shard_map/all_to_all | solution.py:147
  133.0 69.7 %all-gather.3.cloned.1.call-done = bf16[6144,512]{0,1:T(8,128)(2,1)} async-done(((bf16[768,512]{0,1:T(8,128)(2,1)}), bf16[6144,512]{0,1:T(8,128)(2,1)}) %all-gather.3.cloned.1.call-update) | async-done | bytes 6291472 | tf_op jit(solution)/shard_map/all_gather | solution.py:30
  202.7 6.2 %fusion.73 = (bf16[6144,256]{0,1:T(8,128)(2,1)}, bf16[6144,256]{0,1:T(8,128)(2,1)}) fusion(bf16[6144,512]{0,1:T(8,128)(2,1)} %all-gather.3.cloned.1.call-done), kind=kLoop, calls=%fused_computation.86 | loop fusion | bytes 12582912 | tf_op jit(solution)/shard_map/split | solution.py:29
  209.0 69.5 %while.16 = (s32[]{:T(128)}, f32[4,768]{1,0:T(4,128)S(1)}, f32[768,4,64]{0,2,1:T(8,128)S(1)}, s32[]{:T(128)}, bf16[6144,256]{0,1:T(8,128)(2,1)}, /*index=5*/bf16...) while((s32[]{:T(128)}, f32[4,768]{1,0:T(4,128)S(1)}, ...), condition=%wide.region_4.5_spmd.clone, body=%wide.region_0.4_spmd.clone.sunk | while | flops 420745472 | bytes 17461568 | solution.py:68
  209.0 5.8 %conditional.3 = ((f32[4,768]{1,0:T(4,128)S(1)}, f32[768,4,64]{0,2,1:T(8,128)S(1)})) conditional(s32[]{:T(128)} %convert_element_type.106, (f32[4,768]{1,0:T(4,128)S(1)}, f32[768,4,64]{0,2,1:T(8,128)S(1)}) %tuple.51, (s32[]{:T(128)}, s32[]{:T(128)}, bf16[6144,256]{0,1:T(8,128)(2,1)}, bf16[768,4,64]{0,2,1:T(8,128)(2,1)S(1)}, f32[4,768]{1,0:T(4,128)S(1)}, ...), branch_computations={%region_1.0_spmd, %region_2.3_spmd} | conditional | flops 420745472 | bytes 17458250 | solution.py:66
  209.4 1.1 constant_dynamic-slice_fusion
  210.4 1.9 fusion.2
  212.4 2.4 fusion.6
  214.8 5.7 %conditional.3 = ((f32[4,768]{1,0:T(4,128)S(1)}, f32[768,4,64]{0,2,1:T(8,128)S(1)})) conditional(s32[]{:T(128)} %convert_element_type.106, (f32[4,768]{1,0:T(4,128)S(1)}, f32[768,4,64]{0,2,1:T(8,128)S(1)}) %tuple.51, (s32[]{:T(128)}, s32[]{:T(128)}, bf16[6144,256]{0,1:T(8,128)(2,1)}, bf16[768,4,64]{0,2,1:T(8,128)(2,1)S(1)}, f32[4,768]{1,0:T(4,128)S(1)}, ...), branch_computations={%region_1.0_spmd, %region_2.3_spmd} | conditional | flops 420745472 | bytes 17458250 | solution.py:66
  215.2 1.1 constant_dynamic-slice_fusion
  216.2 1.9 fusion.2
  218.2 2.4 fusion.6
  220.6 5.7 %conditional.3 = ((f32[4,768]{1,0:T(4,128)S(1)}, f32[768,4,64]{0,2,1:T(8,128)S(1)})) conditional(s32[]{:T(128)} %convert_element_type.106, (f32[4,768]{1,0:T(4,128)S(1)}, f32[768,4,64]{0,2,1:T(8,128)S(1)}) %tuple.51, (s32[]{:T(128)}, s32[]{:T(128)}, bf16[6144,256]{0,1:T(8,128)(2,1)}, bf16[768,4,64]{0,2,1:T(8,128)(2,1)S(1)}, f32[4,768]{1,0:T(4,128)S(1)}, ...), branch_computations={%region_1.0_spmd, %region_2.3_spmd} | conditional | flops 420745472 | bytes 17458250 | solution.py:66
  221.0 1.1 constant_dynamic-slice_fusion
  222.0 1.9 fusion.2
  224.0 2.4 fusion.6
  226.4 5.7 %conditional.3 = ((f32[4,768]{1,0:T(4,128)S(1)}, f32[768,4,64]{0,2,1:T(8,128)S(1)})) conditional(s32[]{:T(128)} %convert_element_type.106, (f32[4,768]{1,0:T(4,128)S(1)}, f32[768,4,64]{0,2,1:T(8,128)S(1)}) %tuple.51, (s32[]{:T(128)}, s32[]{:T(128)}, bf16[6144,256]{0,1:T(8,128)(2,1)}, bf16[768,4,64]{0,2,1:T(8,128)(2,1)S(1)}, f32[4,768]{1,0:T(4,128)S(1)}, ...), branch_computations={%region_1.0_spmd, %region_2.3_spmd} | conditional | flops 420745472 | bytes 17458250 | solution.py:66
  226.7 1.1 constant_dynamic-slice_fusion
  227.8 1.9 fusion.2
  229.7 2.4 fusion.6
  232.2 5.7 %conditional.3 = ((f32[4,768]{1,0:T(4,128)S(1)}, f32[768,4,64]{0,2,1:T(8,128)S(1)})) conditional(s32[]{:T(128)} %convert_element_type.106, (f32[4,768]{1,0:T(4,128)S(1)}, f32[768,4,64]{0,2,1:T(8,128)S(1)}) %tuple.51, (s32[]{:T(128)}, s32[]{:T(128)}, bf16[6144,256]{0,1:T(8,128)(2,1)}, bf16[768,4,64]{0,2,1:T(8,128)(2,1)S(1)}, f32[4,768]{1,0:T(4,128)S(1)}, ...), branch_computations={%region_1.0_spmd, %region_2.3_spmd} | conditional | flops 420745472 | bytes 17458250 | solution.py:66
  232.5 1.1 constant_dynamic-slice_fusion
  233.6 1.9 fusion.2
  235.5 2.4 fusion.6
  238.0 5.7 %conditional.3 = ((f32[4,768]{1,0:T(4,128)S(1)}, f32[768,4,64]{0,2,1:T(8,128)S(1)})) conditional(s32[]{:T(128)} %convert_element_type.106, (f32[4,768]{1,0:T(4,128)S(1)}, f32[768,4,64]{0,2,1:T(8,128)S(1)}) %tuple.51, (s32[]{:T(128)}, s32[]{:T(128)}, bf16[6144,256]{0,1:T(8,128)(2,1)}, bf16[768,4,64]{0,2,1:T(8,128)(2,1)S(1)}, f32[4,768]{1,0:T(4,128)S(1)}, ...), branch_computations={%region_1.0_spmd, %region_2.3_spmd} | conditional | flops 420745472 | bytes 17458250 | solution.py:66
  238.3 1.1 constant_dynamic-slice_fusion
  239.4 1.9 fusion.2
  241.3 2.4 fusion.6
  243.7 5.7 %conditional.3 = ((f32[4,768]{1,0:T(4,128)S(1)}, f32[768,4,64]{0,2,1:T(8,128)S(1)})) conditional(s32[]{:T(128)} %convert_element_type.106, (f32[4,768]{1,0:T(4,128)S(1)}, f32[768,4,64]{0,2,1:T(8,128)S(1)}) %tuple.51, (s32[]{:T(128)}, s32[]{:T(128)}, bf16[6144,256]{0,1:T(8,128)(2,1)}, bf16[768,4,64]{0,2,1:T(8,128)(2,1)S(1)}, f32[4,768]{1,0:T(4,128)S(1)}, ...), branch_computations={%region_1.0_spmd, %region_2.3_spmd} | conditional | flops 420745472 | bytes 17458250 | solution.py:66
  244.1 1.1 constant_dynamic-slice_fusion
  245.2 1.9 fusion.2
  247.1 2.4 fusion.6
  249.5 5.7 %conditional.3 = ((f32[4,768]{1,0:T(4,128)S(1)}, f32[768,4,64]{0,2,1:T(8,128)S(1)})) conditional(s32[]{:T(128)} %convert_element_type.106, (f32[4,768]{1,0:T(4,128)S(1)}, f32[768,4,64]{0,2,1:T(8,128)S(1)}) %tuple.51, (s32[]{:T(128)}, s32[]{:T(128)}, bf16[6144,256]{0,1:T(8,128)(2,1)}, bf16[768,4,64]{0,2,1:T(8,128)(2,1)S(1)}, f32[4,768]{1,0:T(4,128)S(1)}, ...), branch_computations={%region_1.0_spmd, %region_2.3_spmd} | conditional | flops 420745472 | bytes 17458250 | solution.py:66
  249.9 1.1 constant_dynamic-slice_fusion
  251.0 1.9 fusion.2
  252.9 2.4 fusion.6
  255.3 5.7 %conditional.3 = ((f32[4,768]{1,0:T(4,128)S(1)}, f32[768,4,64]{0,2,1:T(8,128)S(1)})) conditional(s32[]{:T(128)} %convert_element_type.106, (f32[4,768]{1,0:T(4,128)S(1)}, f32[768,4,64]{0,2,1:T(8,128)S(1)}) %tuple.51, (s32[]{:T(128)}, s32[]{:T(128)}, bf16[6144,256]{0,1:T(8,128)(2,1)}, bf16[768,4,64]{0,2,1:T(8,128)(2,1)S(1)}, f32[4,768]{1,0:T(4,128)S(1)}, ...), branch_computations={%region_1.0_spmd, %region_2.3_spmd} | conditional | flops 420745472 | bytes 17458250 | solution.py:66
  256.8 1.9 fusion.2
  258.7 2.4 fusion.6
  261.1 5.7 %conditional.3 = ((f32[4,768]{1,0:T(4,128)S(1)}, f32[768,4,64]{0,2,1:T(8,128)S(1)})) conditional(s32[]{:T(128)} %convert_element_type.106, (f32[4,768]{1,0:T(4,128)S(1)}, f32[768,4,64]{0,2,1:T(8,128)S(1)}) %tuple.51, (s32[]{:T(128)}, s32[]{:T(128)}, bf16[6144,256]{0,1:T(8,128)(2,1)}, bf16[768,4,64]{0,2,1:T(8,128)(2,1)S(1)}, f32[4,768]{1,0:T(4,128)S(1)}, ...), branch_computations={%region_1.0_spmd, %region_2.3_spmd} | conditional | flops 420745472 | bytes 17458250 | solution.py:66
  262.6 1.9 fusion.2
  264.5 2.4 fusion.6
  266.9 5.7 %conditional.3 = ((f32[4,768]{1,0:T(4,128)S(1)}, f32[768,4,64]{0,2,1:T(8,128)S(1)})) conditional(s32[]{:T(128)} %convert_element_type.106, (f32[4,768]{1,0:T(4,128)S(1)}, f32[768,4,64]{0,2,1:T(8,128)S(1)}) %tuple.51, (s32[]{:T(128)}, s32[]{:T(128)}, bf16[6144,256]{0,1:T(8,128)(2,1)}, bf16[768,4,64]{0,2,1:T(8,128)(2,1)S(1)}, f32[4,768]{1,0:T(4,128)S(1)}, ...), branch_computations={%region_1.0_spmd, %region_2.3_spmd} | conditional | flops 420745472 | bytes 17458250 | solution.py:66
  267.3 1.1 constant_dynamic-slice_fusion
  268.3 1.9 fusion.2
  270.3 2.4 fusion.6
  272.7 5.7 %conditional.3 = ((f32[4,768]{1,0:T(4,128)S(1)}, f32[768,4,64]{0,2,1:T(8,128)S(1)})) conditional(s32[]{:T(128)} %convert_element_type.106, (f32[4,768]{1,0:T(4,128)S(1)}, f32[768,4,64]{0,2,1:T(8,128)S(1)}) %tuple.51, (s32[]{:T(128)}, s32[]{:T(128)}, bf16[6144,256]{0,1:T(8,128)(2,1)}, bf16[768,4,64]{0,2,1:T(8,128)(2,1)S(1)}, f32[4,768]{1,0:T(4,128)S(1)}, ...), branch_computations={%region_1.0_spmd, %region_2.3_spmd} | conditional | flops 420745472 | bytes 17458250 | solution.py:66
  274.1 1.9 fusion.2
  276.1 2.4 fusion.6
  279.6 2.0 gather_fusion.1
  282.6 1.6 add_convert_fusion
  (136 shorter events, 14.0 us)
Async XLA Ops:
  8.0 84.1 %copy-start = (bf16[128,2048]{1,0:T(8,128)(2,1)S(1)}, bf16[128,2048]{1,0:T(8,128)(2,1)}, u32[]{:S(2)}) copy-start(bf16[128,2048]{1,0:T(8,128)(2,1)} %param.33) | copy-start | bytes 1572868
  8.0 65.0 %all-gather.5.cloned.1.call-start = ((), (), s32[]{:S(2)}) async-start(), calls=%async_computation.6 | async-start | bytes 3932160 | tf_op jit(solution)/shard_map/all_gather | solution.py:128
  42.6 84.9 %reduce-scatter.5.cloned.1.call-start = ((), (), s32[]{:S(2)}) async-start(), calls=%async_computation.7 | async-start | bytes 3932160 | tf_op jit(solution)/shard_map/reduce_scatter | solution.py:140
  86.1 4.2 %copy-start.3 = (bf16[768,256]{1,0:T(8,128)(2,1)S(1)}, bf16[768,256]{1,0:T(8,128)(2,1)}, u32[]{:S(2)}) copy-start(bf16[768,256]{1,0:T(8,128)(2,1)} %param.21) | copy-start | bytes 1179652
  86.1 4.4 %copy-start.4 = (bf16[768,256]{1,0:T(8,128)(2,1)S(1)}, bf16[768,256]{1,0:T(8,128)(2,1)}, u32[]{:S(2)}) copy-start(bf16[768,256]{1,0:T(8,128)(2,1)} %param.20) | copy-start | bytes 1179652
  90.2 1.5 copy-start.1
  90.2 1.8 copy-start.2
  90.3 3.6 %copy-start.6 = (f32[768,4]{0,1:T(4,128)S(1)}, f32[768,4]{0,1:T(4,128)}, u32[]{:S(2)}) copy-start(f32[768,4]{0,1:T(4,128)} %param.22) | copy-start | bytes 36868
  90.3 29.3 %copy-start.8 = (f32[256]{0:T(256)S(1)}, f32[256]{0:T(256)}, u32[]{:S(2)}) copy-start(f32[256]{0:T(256)} %param.23) | copy-start | bytes 3076
  90.3 29.3 %copy-start.7 = (f32[128,4]{0,1:T(4,128)S(1)}, f32[128,4]{0,1:T(4,128)}, u32[]{:S(2)}) copy-start(f32[128,4]{0,1:T(4,128)} %param.27) | copy-start | bytes 6148
  90.3 112.4 %all-gather.3.cloned.1.call-start = ((), (), s32[]{:S(2)}) async-start(), calls=%async_computation.4 | async-start | bytes 7077888 | tf_op jit(solution)/shard_map/all_gather | solution.py:30
  90.7 3.0 %copy-start.5 = (bf16[768,256]{1,0:T(8,128)(2,1)S(1)}, bf16[768,256]{1,0:T(8,128)(2,1)}, u32[]{:S(2)}) copy-start(bf16[768,256]{1,0:T(8,128)(2,1)} %param.19) | copy-start | bytes 1179652
  91.7 190.9 %reduce-scatter.3.cloned.1.call-start = ((), (), s32[]{:S(2)}) async-start(), calls=%async_computation.5 | async-start | bytes 655360 | tf_op jit(solution)/shard_map/reduce_scatter | solution.py:143
  127.5 152.1 %all-to-all-start.1 = ((bf16[8,96,512]{2,1,0:T(8,128)(2,1)}), bf16[8,96,512]{2,1,0:T(8,128)(2,1)S(1)}, u32[]{:S(2)}, u32[]{:S(2)}) async-start(bf16[8,96,512]{2,1,0:T(8,128)(2,1)} %bitcast.103), calls=%async_computation.3 | async-start | bytes 1572864 | tf_op jit(solution)/shard_map/all_to_all | solution.py:147
Sparse Core Ops, SparseCore 0:
  42.7 30.1 all-gather.4
  90.4 37.1 reduce-scatter.4
  130.0 21.6 reduce-scatter.2
Sparse Core Ops, SparseCore 1:
  93.0 109.6 all-gather.2
